TPU v7x, 512 devices: a whole 4x4x16 slice. The times are simulated.
512 devices in a mesh: fs: 64 (over z, y), tp: 8 (over x, core).
Axes of the slice: x: 4, y: 4, z: 16, core: 2. Of those that a mesh axis runs over, the one named last changes fastest.
Arguments:
- tokens: bfloat16 [16384, 2048], P('fs'), may hold values from -6 to 6
- mix_gain: float32 [2048], replicated, may hold values from 0.1 to 1.9
- glu_value: bfloat16 [2048, 2048], P('fs', 'tp'), may hold values from -0.125 to 0.125
- glu_gate: bfloat16 [2048, 2048], P('fs', 'tp'), may hold values from -0.125 to 0.125
- conv_taps: float32 [31, 2048], P(None, 'tp'), may hold values from -2.2 to 2.2, as said below
- chan_gain: float32 [2048], P('tp'), may hold values from 0.1 to 1.9
- mix_out: bfloat16 [2048, 2048], P('tp', 'fs'), may hold values from -0.125 to 0.125
- mlp_gain: float32 [2048], replicated, may hold values from 0.1 to 1.9
- up_weight: bfloat16 [2048, 8192], P('fs', 'tp'), may hold values from -0.125 to 0.125
- down_weight: bfloat16 [8192, 2048], P('tp', 'fs'), may hold values from -0.0625 to 0.0625
Outputs:
- result: bfloat16 [16384, 2048], P('fs')
Inputs may be any that keep to these rules, and one draw needn't show every extreme that they name: `conv_taps`: independent entries scaled by fan-in; channels fall into 16 groups of different scale.
All inputs are finite; a program needn't handle non-finite values.
Results may differ from a plain program's by a relative error of at most 0.018.
Values may be sent and summed in bfloat16 or wider, within the bound.
A program may use at most 64 MiB of HBM per device.

v0:
```python
import jax
import jax.numpy as jnp
from jax import lax
from jax.sharding import PartitionSpec as P

C = 2048
LEN = 128
norm_floor = 0.05


def in_one_piece(arrays, axis, dim, along):
    widths = [a.shape[along] for a in arrays]
    both = jnp.concatenate(arrays, axis=along)
    result = lax.all_gather(both, axis, axis=dim, tiled=True)
    return tuple(jnp.split(result, [sum(widths[:k]) for k in range(1, len(widths))], axis=along))


def rows_first(arrays, axis, dims):
    turned = [jnp.moveaxis(a, dim, 0) for a, dim in zip(arrays, dims)]
    both = jnp.concatenate([t.reshape(len(t), -1) for t in turned], axis=1)
    result, at, gathered = (lax.all_gather(both, axis, axis=0, tiled=True), 0, [])
    for t, dim in zip(turned, dims):
        piece = result[:, at : at + t[0].size].reshape(-1, *t.shape[1:])
        gathered.append(jnp.moveaxis(piece, 0, dim))
        at += t[0].size
    return tuple(gathered)


def sent_to_all(shard, axis):
    count = lax.axis_size(axis)
    return lax.all_to_all(
        jnp.broadcast_to(shard[None], (count, *shard.shape)), axis, 0, 0, tiled=True
    )


def over_copies(shard, axis):
    everything = sent_to_all(shard, axis)
    return jnp.sum(everything, axis=0)


def together(arrays, axis):
    vector, at, gathered = (jnp.concatenate([a.reshape(-1) for a in arrays]), 0, [])
    running = over_copies(vector, axis)
    for a in arrays:
        gathered.append(running[at : at + a.size].reshape(a.shape))
        at += a.size
    return tuple(gathered)


def in_blocks(shard, dim, count):
    shape = shard.shape
    pieces = shard.reshape(*shape[:dim], count, shape[dim] // count, *shape[dim + 1 :])
    return jnp.moveaxis(pieces, dim, 0)


def summed_on_arrival(shard, axis, dim):
    count = lax.axis_size(axis)
    pieces = lax.all_to_all(in_blocks(shard, dim, count), axis, 0, 0, tiled=True)
    return jnp.sum(pieces.astype(jnp.float32), axis=0)


def joined_along(pieces, dim):
    shape = list(pieces.shape[1:])
    shape[dim] *= pieces.shape[0]
    return jnp.moveaxis(pieces, 0, dim).reshape(shape)


def gather_directly(shard, axis, dim):
    return joined_along(sent_to_all(shard, axis), dim)


def rms_scale(stream, gain):
    return stream * lax.rsqrt(jnp.mean(stream * stream, axis=-1, keepdims=True) + norm_floor) * gain


def bf16_round(value):
    return lax.optimization_barrier(value.astype(jnp.bfloat16)).astype(jnp.float32)


def depthwise(glu, conv_taps):
    seqs = glu.shape[0] // LEN
    blocks = glu.reshape(seqs, LEN, glu.shape[1]).astype(jnp.float32)
    reach = conv_taps.shape[0] // 2
    padded = jnp.pad(blocks, ((0, 0), (reach, reach), (0, 0)))
    total = jnp.zeros_like(blocks)
    for offset in range(conv_taps.shape[0]):
        total = total + padded[:, offset : offset + LEN] * conv_taps[offset]
    return total.reshape(glu.shape)


def per_device(
    tokens,
    mix_gain,
    glu_value,
    glu_gate,
    conv_taps,
    chan_gain,
    mix_out,
    mlp_gain,
    up_weight,
    down_weight,
):
    stream = tokens.astype(jnp.float32)
    normed = rms_scale(stream, mix_gain).astype(jnp.bfloat16)
    row_parts = in_one_piece((glu_value, glu_gate, up_weight), "fs", 0, 1)
    column_parts = rows_first((mix_out, down_weight), "fs", (1, 1))
    values = jnp.dot(normed, row_parts[0], preferred_element_type=jnp.float32)
    gating = jnp.dot(normed, row_parts[1], preferred_element_type=jnp.float32)
    glu = (values * jax.nn.sigmoid(gating)).astype(jnp.bfloat16)
    convolved = depthwise(glu, conv_taps)
    sums, squares = together(
        (jnp.sum(convolved, axis=-1), jnp.sum(convolved * convolved, axis=-1)), "tp"
    )
    centre = (sums / C)[:, None]
    spread = (squares / C)[:, None] - centre * centre
    hidden = jax.nn.silu((convolved - centre) * lax.rsqrt(spread + norm_floor) * chan_gain).astype(
        jnp.bfloat16
    )
    whole_out = column_parts[0]
    own_rows = stream.shape[0] // lax.axis_size("tp")
    mixed = summed_on_arrival(
        jnp.dot(hidden, whole_out, preferred_element_type=jnp.float32).astype(jnp.bfloat16), "tp", 0
    )
    own_stream = lax.dynamic_slice_in_dim(stream, lax.axis_index("tp") * own_rows, own_rows, 0)
    resid = own_stream + bf16_round(mixed)
    normed_mlp = rms_scale(resid, mlp_gain).astype(jnp.bfloat16)
    whole_up = row_parts[2]
    active = jnp.square(
        jax.nn.relu(
            jnp.dot(
                gather_directly(normed_mlp, "tp", 0), whole_up, preferred_element_type=jnp.float32
            )
        )
    ).astype(jnp.bfloat16)
    whole_down = column_parts[1]
    feed = summed_on_arrival(
        jnp.dot(active, whole_down, preferred_element_type=jnp.float32).astype(jnp.bfloat16),
        "tp",
        0,
    )
    finished = (resid + bf16_round(feed)).astype(jnp.bfloat16)
    return gather_directly(finished, "tp", 0)


def solution(mesh):
    in_specs = (
        P("fs", None),
        P(),
        P("fs", "tp"),
        P("fs", "tp"),
        P(None, "tp"),
        P("tp"),
        P("tp", "fs"),
        P(),
        P("fs", "tp"),
        P("tp", "fs"),
    )
    out_specs = P("fs", None)
    return jax.shard_map(
        per_device, mesh=mesh, in_specs=in_specs, out_specs=out_specs, check_vma=False
    )
```

profile of v0, /device:TPU:1, one launch (start us, length us, event | category | flops | bytes accessed | tf_op | source)
XLA Modules:
  0.0 408.4 jit_solution(4157544092094613481)
XLA Ops:
  6.5 0.0 all-gather.3.cloned.1.call-start
  6.5 1.5 pad_maximum_fusion
  8.0 0.0 all-gather.3.cloned.1.call-update
  8.1 0.0 all-gather.5.cloned.1.call-start
  8.1 1.5 pad_maximum_fusion.1
  9.6 0.0 all-gather.5.cloned.1.call-update
  9.6 1.5 multiply_reduce_fusion
  11.1 0.0 copy-start
  11.1 0.0 copy-start.3
  11.2 1.0 fusion.94
  12.1 1.0 fusion.93
  13.2 145.1 %all-gather.3.cloned.1.call-done = bf16[2048,1536]{1,0:T(8,128)(2,1)} async-done(((bf16[32,1536]{1,0:T(8,128)(2,1)}), bf16[2048,1536]{1,0:T(8,128)(2,1)}) %all-gather.3.cloned.1.call-update) | async-done | bytes 6291472 | tf_op jit(solution)/shard_map/all_gather | solution.py:14
  158.3 2.0 fusion.23
  160.3 0.0 copy-done
  160.3 0.0 copy-done.3
  160.4 0.0 copy-start.2
  160.4 1.8 bitcast_convert_fusion
  162.1 1.2 fusion.91
  163.3 17.4 %all_to_all.26 = f32[8,1,512]{2,1,0:T(1,128)S(1)} all-to-all(f32[8,1,512]{2,1,0:T(1,128)S(1)} %broadcast_in_dim.6), channel_id=1, replica_groups=mesh['fs'=64,'tp'=8] {'tp'}, dimensions={0} | all-to-all | bytes 32768 | tf_op jit(solution)/shard_map/all_to_all | solution.py:31
  180.8 0.0 copy-done.2
  180.8 0.2 multiply_convert_fusion.4
  181.0 123.2 %all-gather.5.cloned.1.call-done = bf16[2048,1280]{1,0:T(8,128)(2,1)} async-done(((bf16[32,1280]{1,0:T(8,128)(2,1)}), bf16[2048,1280]{1,0:T(8,128)(2,1)}) %all-gather.5.cloned.1.call-update) | async-done | bytes 5242896 | tf_op jit(solution)/shard_map/all_gather | solution.py:21
  304.2 2.7 convolution_convert_fusion
  306.9 14.1 %all-to-all-start.1 = ((bf16[8,32,2048]{2,1,0:T(8,128)(2,1)}), bf16[8,32,2048]{2,1,0:T(8,128)(2,1)S(1)}, u32[]{:S(2)}, u32[]{:S(2)}) async-start(bf16[8,32,2048]{2,1,0:T(8,128)(2,1)} %bitcast.38), calls=%async_computation.1 | async-start | bytes 2097152 | tf_op jit(solution)/shard_map/all_to_all | solution.py:58
  320.9 0.0 copy-start.1
  320.9 1.7 convert_element_type.45
  322.6 13.3 %all-to-all-done.1 = bf16[8,32,2048]{2,1,0:T(8,128)(2,1)S(1)} async-done(((bf16[8,32,2048]{2,1,0:T(8,128)(2,1)}), bf16[8,32,2048]{2,1,0:T(8,128)(2,1)S(1)}, u32[]{:S(2)}, u32[]{:S(2)}) %all-to-all-start.1) | async-done | bytes 1048608 | tf_op jit(solution)/shard_map/all_to_all | solution.py:58
  335.9 0.1 reduce_sum.79
  336.1 1.1 multiply_reduce_fusion.1
  337.2 0.0 copy-done.1
  337.2 1.0 multiply_convert_fusion.3
  338.2 0.1 broadcast_in_dim.7
  338.4 18.3 %all_to_all.27 = bf16[8,32,2048]{2,1,0:T(8,128)(2,1)S(1)} all-to-all(bf16[8,32,2048]{2,1,0:T(8,128)(2,1)S(1)} %broadcast_in_dim.7), channel_id=1, replica_groups=mesh['fs'=64,'tp'=8] {'tp'}, dimensions={0} | all-to-all | bytes 2097152 | tf_op jit(solution)/shard_map/all_to_all | solution.py:31
  356.7 5.8 %fusion.4 = bf16[256,2048]{1,0:T(8,128)(2,1)S(1)} fusion(bf16[2048,1280]{1,0:T(8,128)(2,1)} %all-gather.5.cloned.1.call-done, bf16[256,2048]{1,0:T(8,128)(2,1)S(1)} %bitcast.53, bf16[2048,1536]{1,0:T(8,128)(2,1)} %all-gather.3.cloned.1.call-done), kind=kOutput, calls=%fused_computation.4 | convolution fusion | flops 2148794368 | bytes 10485760 | tf_op jit(solution)/shard_map/dot_general | solution.py:137
  362.5 18.4 %all_to_all.28 = bf16[8,32,2048]{2,1,0:T(8,128)(2,1)S(1)} all-to-all(bf16[8,32,2048]{2,1,0:T(8,128)(2,1)S(1)} %bitcast.54), channel_id=1, replica_groups=mesh['fs'=64,'tp'=8] {'tp'}, dimensions={0} | all-to-all | bytes 2097152 | tf_op jit(solution)/shard_map/all_to_all | solution.py:58
  380.9 0.1 reduce_sum.81
  381.0 1.0 add_convert_fusion
  382.0 0.1 broadcast_in_dim.8
  382.2 18.4 %all_to_all.29 = bf16[8,32,2048]{2,1,0:T(8,128)(2,1)S(1)} all-to-all(bf16[8,32,2048]{2,1,0:T(8,128)(2,1)S(1)} %broadcast_in_dim.8), channel_id=1, replica_groups=mesh['fs'=64,'tp'=8] {'tp'}, dimensions={0} | all-to-all | bytes 2097152 | tf_op jit(solution)/shard_map/all_to_all | solution.py:31
  400.6 1.0 copy.16
  (6 shorter events, 0.1 us)
Async XLA Ops:
  6.5 151.8 %all-gather.3.cloned.1.call-start = ((), (), s32[]{:S(2)}) async-start(), calls=%async_computation.5 | async-start | bytes 6389760 | tf_op jit(solution)/shard_map/all_gather | solution.py:14
  8.1 296.2 %all-gather.5.cloned.1.call-start = ((), (), s32[]{:S(2)}) async-start(), calls=%async_computation.6 | async-start | bytes 5324800 | tf_op jit(solution)/shard_map/all_gather | solution.py:21
  11.1 149.2 %copy-start = (bf16[256,2048]{1,0:T(8,128)(2,1)S(1)}, bf16[256,2048]{1,0:T(8,128)(2,1)}, u32[]{:S(2)}) copy-start(bf16[256,2048]{1,0:T(8,128)(2,1)} %param.10) | copy-start | bytes 3145732
  11.1 149.2 %copy-start.3 = (f32[2048]{0:T(1024)S(1)}, f32[2048]{0:T(1024)}, u32[]{:S(2)}) copy-start(f32[2048]{0:T(1024)} %param.11) | copy-start | bytes 24580
  160.4 20.4 %copy-start.2 = (f32[256]{0:T(256)S(1)}, f32[256]{0:T(256)}, u32[]{:S(2)}) copy-start(f32[256]{0:T(256)} %param.15) | copy-start | bytes 3076
  306.9 29.0 %all-to-all-start.1 = ((bf16[8,32,2048]{2,1,0:T(8,128)(2,1)}), bf16[8,32,2048]{2,1,0:T(8,128)(2,1)S(1)}, u32[]{:S(2)}, u32[]{:S(2)}) async-start(bf16[8,32,2048]{2,1,0:T(8,128)(2,1)} %bitcast.38), calls=%async_computation.1 | async-start | bytes 2097152 | tf_op jit(solution)/shard_map/all_to_all | solution.py:58
  320.9 16.2 %copy-start.1 = (f32[2048]{0:T(1024)S(1)}, f32[2048]{0:T(1024)}, u32[]{:S(2)}) copy-start(f32[2048]{0:T(1024)} %param.17) | copy-start | bytes 24580
Sparse Core Ops, SparseCore 0:
  10.3 147.9 all-gather.2
  161.2 142.9 all-gather.4
where the time goes:
time: 409 us; the launch traced here: 408 us
  waiting for transfers between devices  282 us (69%)
  blocking collectives  72.5 us (18%)
  starting transfers between devices  14.1 us (3%)
  between operations  13.5 us (3%)
  matrix products  12.3 us (3%)
  other arithmetic  11 us (3%)
    all_gather x1, waiting for transfers between devices, in_one_piece(): result = lax.all_gather(both, axis, axis=dim, tiled=True)  145 us
    all_gather x1, waiting for transfers between devices, rows_first(): lax.all_gather(both, axis, axis=0, tiled=True)  123 us
    all_to_all x3, blocking collectives, sent_to_all(): lax.all_to_all(jnp.broadcast_to(shard[None], (count, *shard.shape)), axis...  54.1 us
    all_to_all x1, blocking collectives, summed_on_arrival(): lax.all_to_all(in_blocks(shard, dim, count), axis, 0, 0, tiled=True)  18.4 us
    all_to_all x1, starting transfers between devices, summed_on_arrival(): lax.all_to_all(in_blocks(shard, dim, count), axis, 0, 0, tiled=True)  14.1 us
    all_to_all x1, waiting for transfers between devices, summed_on_arrival(): lax.all_to_all(in_blocks(shard, dim, count), axis, 0, 0, tiled=True)  13.3 us
  transfers between devices with their start and end apart: 3, of which 3 were waited for; matrix products, arithmetic and copies ran while one was open for 3% of the time, Pallas kernels for 0%

commit v1 on v0

--- a/solution.py
+++ b/solution.py
@@ -18,7 +18,13 @@
 def rows_first(arrays, axis, dims):
     turned = [jnp.moveaxis(a, dim, 0) for a, dim in zip(arrays, dims)]
     both = jnp.concatenate([t.reshape(len(t), -1) for t in turned], axis=1)
-    result, at, gathered = (lax.all_gather(both, axis, axis=0, tiled=True), 0, [])
+    result, at, gathered = (
+        jnp.concatenate(
+            lax.all_to_all(jnp.stack([both] * lax.axis_size(axis)), axis, 0, 0), axis=0
+        ),
+        0,
+        [],
+    )
     for t, dim in zip(turned, dims):
         piece = result[:, at : at + t[0].size].reshape(-1, *t.shape[1:])
         gathered.append(jnp.moveaxis(piece, 0, dim))

time: 409 us -> 524 us (1.28)
  waiting for transfers between devices: 282 us -> 391 us
  starting transfers between devices: 14.1 us -> 35 us
  blocking collectives: 72.5 us -> 55.1 us
    all_to_all x0 -> x2, waiting for transfers between devices: none -> 231 us  [the longest x1 227 us: rows_first(): lax.all_to_all(jnp.stack([both] * lax.axis_size(axis)), axis, 0, 0)]
    all_gather x1 -> x0, waiting for transfers between devices: 123 us -> none  [rows_first(): lax.all_gather(both, axis, axis=0, tiled=True)]
    all_to_all x0 -> x2, starting transfers between devices: none -> 22.7 us  [the longest x1 13 us: sent_to_all(): lax.all_to_all(jnp.broadcast_to(shard[None], (count, *shard.shape)), axis...]
    all_to_all x3 -> x2, blocking collectives: 54.1 us -> 36.7 us  [sent_to_all(): lax.all_to_all(jnp.broadcast_to(shard[None], (count, *shard.shape)), axis...]
  transfers between devices with their start and end apart: 3 -> 4, of which waited for: 3 -> 4; matrix products, arithmetic and copies ran while one was open for 3% -> 1% of each run, Pallas kernels for 0% -> 0%
where the time goes in v1:
time: 524 us
  waiting for transfers between devices  391 us (75%)
  blocking collectives  55.1 us (11%)
  starting transfers between devices  35 us (7%)
  between operations  13.5 us (3%)
  matrix products  12.3 us (2%)
  other arithmetic  9.66 us (2%)
  local copies, waits for them, and re-layouts  6.74 us (1%)
    all_to_all x1, waiting for transfers between devices, rows_first(): lax.all_to_all(jnp.stack([both] * lax.axis_size(axis)), axis, 0, 0)  227 us
    all_gather x1, waiting for transfers between devices, in_one_piece(): result = lax.all_gather(both, axis, axis=dim, tiled=True)  147 us
    all_to_all x2, blocking collectives, sent_to_all(): lax.all_to_all(jnp.broadcast_to(shard[None], (count, *shard.shape)), axis...  36.7 us
    all_to_all x1, blocking collectives, summed_on_arrival(): lax.all_to_all(in_blocks(shard, dim, count), axis, 0, 0, tiled=True)  18.4 us
    all_to_all x1, waiting for transfers between devices, summed_on_arrival(): lax.all_to_all(in_blocks(shard, dim, count), axis, 0, 0, tiled=True)  13.3 us
    all_to_all x1, starting transfers between devices, sent_to_all(): lax.all_to_all(jnp.broadcast_to(shard[None], (count, *shard.shape)), axis...  13 us
    all_to_all x1, starting transfers between devices, summed_on_arrival(): lax.all_to_all(in_blocks(shard, dim, count), axis, 0, 0, tiled=True)  12.3 us
  transfers between devices with their start and end apart: 4, of which 4 were waited for; matrix products, arithmetic and copies ran while one was open for 1% of the time, Pallas kernels for 0%

profile of v1, /device:TPU:1, one launch (start us, length us, event | category | flops | bytes accessed | tf_op | source)
XLA Modules:
  0.0 523.7 jit_solution(14273237429983482215)
XLA Ops:
  6.5 0.0 copy-start
  6.5 0.0 copy-start.5
  6.5 0.0 all-gather.2.cloned.1.call-start
  6.5 1.6 pad_maximum_fusion
  8.1 0.0 all-gather.2.cloned.1.call-update
  8.1 1.5 multiply_reduce_fusion
  9.7 1.0 fusion.94
  10.6 1.0 fusion.93
  11.7 0.0 copy-start.1
  11.7 0.0 copy-start.2
  11.7 146.6 %all-gather.2.cloned.1.call-done = bf16[2048,1536]{1,0:T(8,128)(2,1)} async-done(((bf16[32,1536]{1,0:T(8,128)(2,1)}), bf16[2048,1536]{1,0:T(8,128)(2,1)}) %all-gather.2.cloned.1.call-update) | async-done | bytes 6291472 | tf_op jit(solution)/shard_map/all_gather | solution.py:14
  158.3 2.0 fusion.23
  160.3 0.0 copy-done
  160.4 0.0 copy-done.5
  160.4 1.7 bitcast_convert_fusion
  162.1 1.2 fusion.91
  163.3 0.6 broadcast_in_dim.6
  163.9 13.0 %all-to-all-start = ((f32[8,1,512]{2,1,0:T(1,128)}), f32[8,1,512]{2,1,0:T(1,128)S(1)}, u32[]{:S(2)}, u32[]{:S(2)}) async-start(f32[8,1,512]{2,1,0:T(1,128)} %broadcast_in_dim.6), calls=%async_computation | async-start | bytes 32768 | tf_op jit(solution)/shard_map/all_to_all | solution.py:37
  176.9 0.0 copy-done.1
  176.9 0.0 copy-done.2
  176.9 4.6 all-to-all-done
  181.6 2.9 stack.2
  184.5 0.0 copy-start.4
  184.5 9.7 %all-to-all-start.1 = ((bf16[64,32,1280]{2,1,0:T(8,128)(2,1)}), bf16[64,32,1280]{2,1,0:T(8,128)(2,1)}, u32[]{:S(2)}, u32[]{:S(2)}) async-start(bf16[64,32,1280]{2,1,0:T(8,128)(2,1)} %stack.2), calls=%async_computation.1 | async-start | bytes 10485760 | tf_op jit(solution)/shard_map/all_to_all | solution.py:23
  194.2 0.0 copy-done.4
  194.3 0.2 multiply_convert_fusion.4
  194.4 226.8 %all-to-all-done.1 = bf16[64,32,1280]{2,1,0:T(8,128)(2,1)} async-done(((bf16[64,32,1280]{2,1,0:T(8,128)(2,1)}), bf16[64,32,1280]{2,1,0:T(8,128)(2,1)}, u32[]{:S(2)}, u32[]{:S(2)}) %all-to-all-start.1) | async-done | bytes 5242912 | tf_op jit(solution)/shard_map/all_to_all | solution.py:23
  421.2 0.0 copy-start.3
  421.2 2.7 convolution_convert_fusion
  423.9 12.3 %all-to-all-start.2 = ((bf16[8,32,2048]{2,1,0:T(8,128)(2,1)}), bf16[8,32,2048]{2,1,0:T(8,128)(2,1)S(1)}, u32[]{:S(2)}, u32[]{:S(2)}) async-start(bf16[8,32,2048]{2,1,0:T(8,128)(2,1)} %bitcast.39), calls=%async_computation.2 | async-start | bytes 2097152 | tf_op jit(solution)/shard_map/all_to_all | solution.py:64
  436.2 1.7 convert_element_type.45
  437.9 13.3 %all-to-all-done.2 = bf16[8,32,2048]{2,1,0:T(8,128)(2,1)S(1)} async-done(((bf16[8,32,2048]{2,1,0:T(8,128)(2,1)}), bf16[8,32,2048]{2,1,0:T(8,128)(2,1)S(1)}, u32[]{:S(2)}, u32[]{:S(2)}) %all-to-all-start.2) | async-done | bytes 1048608 | tf_op jit(solution)/shard_map/all_to_all | solution.py:64
  451.2 0.1 reduce_sum.79
  451.4 1.1 multiply_reduce_fusion.1
  452.5 0.0 copy-done.3
  452.5 1.1 multiply_convert_fusion.3
  453.6 0.1 broadcast_in_dim.7
  453.7 18.3 %all_to_all.31 = bf16[8,32,2048]{2,1,0:T(8,128)(2,1)S(1)} all-to-all(bf16[8,32,2048]{2,1,0:T(8,128)(2,1)S(1)} %broadcast_in_dim.7), channel_id=1, replica_groups=mesh['fs'=64,'tp'=8] {'tp'}, dimensions={0} | all-to-all | bytes 2097152 | tf_op jit(solution)/shard_map/all_to_all | solution.py:37
  472.0 5.8 %fusion.4 = bf16[256,2048]{1,0:T(8,128)(2,1)S(1)} fusion(bf16[2048,1280]{1,0:T(8,128)(2,1)} %bitcast.38, bf16[256,2048]{1,0:T(8,128)(2,1)S(1)} %bitcast.54, bf16[2048,1536]{1,0:T(8,128)(2,1)} %all-gather.2.cloned.1.call-done), kind=kOutput, calls=%fused_computation.4 | convolution fusion | flops 2148794368 | bytes 10485760 | tf_op jit(solution)/shard_map/dot_general | solution.py:143
  477.8 18.4 %all_to_all.32 = bf16[8,32,2048]{2,1,0:T(8,128)(2,1)S(1)} all-to-all(bf16[8,32,2048]{2,1,0:T(8,128)(2,1)S(1)} %bitcast.55), channel_id=1, replica_groups=mesh['fs'=64,'tp'=8] {'tp'}, dimensions={0} | all-to-all | bytes 2097152 | tf_op jit(solution)/shard_map/all_to_all | solution.py:64
  496.2 0.1 reduce_sum.81
  496.4 1.0 add_convert_fusion
  497.4 0.1 broadcast_in_dim.8
  497.5 18.4 %all_to_all.33 = bf16[8,32,2048]{2,1,0:T(8,128)(2,1)S(1)} all-to-all(bf16[8,32,2048]{2,1,0:T(8,128)(2,1)S(1)} %broadcast_in_dim.8), channel_id=1, replica_groups=mesh['fs'=64,'tp'=8] {'tp'}, dimensions={0} | all-to-all | bytes 2097152 | tf_op jit(solution)/shard_map/all_to_all | solution.py:37
  515.9 1.0 copy.16
  (6 shorter events, 0.1 us)
Async XLA Ops:
  6.5 153.8 %copy-start = (bf16[256,2048]{1,0:T(8,128)(2,1)S(1)}, bf16[256,2048]{1,0:T(8,128)(2,1)}, u32[]{:S(2)}) copy-start(bf16[256,2048]{1,0:T(8,128)(2,1)} %param.10) | copy-start | bytes 3145732
  6.5 153.8 %copy-start.5 = (f32[2048]{0:T(1024)S(1)}, f32[2048]{0:T(1024)}, u32[]{:S(2)}) copy-start(f32[2048]{0:T(1024)} %param.11) | copy-start | bytes 24580
  6.5 151.8 %all-gather.2.cloned.1.call-start = ((), (), s32[]{:S(2)}) async-start(), calls=%async_computation.6 | async-start | bytes 6389760 | tf_op jit(solution)/shard_map/all_gather | solution.py:14
  11.7 165.2 %copy-start.1 = (bf16[1024,32]{0,1:T(8,128)(2,1)S(1)}, bf16[1024,32]{0,1:T(8,128)(2,1)}, u32[]{:S(2)}) copy-start(bf16[1024,32]{0,1:T(8,128)(2,1)} %param.19) | copy-start | bytes 196612
  11.7 165.2 %copy-start.2 = (bf16[256,32]{0,1:T(8,128)(2,1)S(1)}, bf16[256,32]{0,1:T(8,128)(2,1)}, u32[]{:S(2)}) copy-start(bf16[256,32]{0,1:T(8,128)(2,1)} %param.16) | copy-start | bytes 49156
  163.9 17.6 %all-to-all-start = ((f32[8,1,512]{2,1,0:T(1,128)}), f32[8,1,512]{2,1,0:T(1,128)S(1)}, u32[]{:S(2)}, u32[]{:S(2)}) async-start(f32[8,1,512]{2,1,0:T(1,128)} %broadcast_in_dim.6), calls=%async_computation | async-start | bytes 32768 | tf_op jit(solution)/shard_map/all_to_all | solution.py:37
  184.5 9.8 %copy-start.4 = (f32[256]{0:T(256)S(1)}, f32[256]{0:T(256)}, u32[]{:S(2)}) copy-start(f32[256]{0:T(256)} %param.15) | copy-start | bytes 3076
  184.5 236.8 %all-to-all-start.1 = ((bf16[64,32,1280]{2,1,0:T(8,128)(2,1)}), bf16[64,32,1280]{2,1,0:T(8,128)(2,1)}, u32[]{:S(2)}, u32[]{:S(2)}) async-start(bf16[64,32,1280]{2,1,0:T(8,128)(2,1)} %stack.2), calls=%async_computation.1 | async-start | bytes 10485760 | tf_op jit(solution)/shard_map/all_to_all | solution.py:23
  421.2 31.3 %copy-start.3 = (f32[2048]{0:T(1024)S(1)}, f32[2048]{0:T(1024)}, u32[]{:S(2)}) copy-start(f32[2048]{0:T(1024)} %param.17) | copy-start | bytes 24580
  423.9 27.3 %all-to-all-start.2 = ((bf16[8,32,2048]{2,1,0:T(8,128)(2,1)}), bf16[8,32,2048]{2,1,0:T(8,128)(2,1)S(1)}, u32[]{:S(2)}, u32[]{:S(2)}) async-start(bf16[8,32,2048]{2,1,0:T(8,128)(2,1)} %bitcast.39), calls=%async_computation.2 | async-start | bytes 2097152 | tf_op jit(solution)/shard_map/all_to_all | solution.py:64
Sparse Core Ops, SparseCore 0:
  10.3 147.9 all-gather.1
